TPU v7x, 32 devices: a whole 2x2x4 slice. The times are simulated.
32 devices in a mesh: grp: 2 (over y), ra: 4 (over z), cb: 4 (over x, core).
Axes of the slice: x: 2, y: 2, z: 4, core: 2. Of those that a mesh axis runs over, the one named last changes fastest.
Arguments:
- tokens: bfloat16 [256, 2048], P('grp', 'ra'), parts along dimension 0, may hold values from -8 to 8
- first_gain: bfloat16 [2048], P('ra'), may hold values from 0.099609375 to 1.8984375
- first_gate: bfloat16 [2048, 5632], P('ra', 'cb'), may hold values from -0.125 to 0.125
- first_up: bfloat16 [2048, 5632], P('ra', 'cb'), may hold values from -0.125 to 0.125
- first_down: bfloat16 [5632, 2048], P('cb', 'ra'), may hold values from -0.078125 to 0.078125
- second_gain: bfloat16 [2048], P('ra'), may hold values from 0.099609375 to 1.8984375
- second_gate: bfloat16 [2048, 5632], P('ra', 'cb'), may hold values from -0.125 to 0.125
- second_up: bfloat16 [2048, 5632], P('ra', 'cb'), may hold values from -0.125 to 0.125
- second_down: bfloat16 [5632, 2048], P('cb', 'ra'), may hold values from -0.078125 to 0.078125
Outputs:
- latent_out: bfloat16 [256, 2048], P('grp', 'ra'), parts along dimension 0
There are 2 independent parts, one for each index of `grp`. A program takes and returns all parts, laid end to end along the dimension named above; an argument that names none is the same for every part. Nothing has to cross between parts.
All inputs are finite; a program needn't handle non-finite values.
Results may differ from a plain program's by a relative error of at most 0.0088.
Values may be sent and summed in bfloat16 or wider, within the bound.
No kernel may reach another device: no remote copies, remote signals or barrier semaphores. Data moves between devices by JAX's collectives and lax.ppermute only.
A program may use at most 64 MiB of HBM per device.

v0:
```python
import jax
import jax.numpy as jnp
from jax import lax
from jax.sharding import PartitionSpec as P


def sublayer(x, gain, w_gate, w_up, w_down):
    xf = x.astype(jnp.float32)
    width = x.shape[1] * lax.axis_size("ra")
    rows = x.shape[0]
    squares = jnp.sum(xf * xf, axis=1)
    normed = (xf * gain.astype(jnp.float32)).astype(jnp.bfloat16)
    dims = (((0,), (1,)), ((), ()))
    gate_rows = lax.dot_general(w_gate, normed, dims, preferred_element_type=jnp.float32)
    up_rows = lax.dot_general(w_up, normed, dims, preferred_element_type=jnp.float32)
    shares = lax.psum_scatter(
        jnp.concatenate([gate_rows, up_rows], axis=1), "ra", scatter_dimension=0, tiled=True
    )
    total_sq = lax.psum(squares, "ra")
    scale = lax.rsqrt(total_sq / width + 1e-06)
    hidden_t = (
        jax.nn.silu(shares[:, :rows] * scale[None, :]) * (shares[:, rows:] * scale[None, :])
    ).astype(jnp.bfloat16)
    partial_value = lax.dot_general(
        lax.all_gather(hidden_t, "ra", axis=0, tiled=True),
        w_down,
        (((0,), (0,)), ((), ())),
        preferred_element_type=jnp.float32,
    )
    branch = lax.psum(partial_value, "cb")
    return (0.5 * xf + 0.5 * branch).astype(jnp.bfloat16)


def per_device(
    tokens,
    first_gain,
    first_gate,
    first_up,
    first_down,
    second_gain,
    second_gate,
    second_up,
    second_down,
):
    middle = sublayer(tokens, first_gain, first_gate, first_up, first_down)
    return sublayer(middle, second_gain, second_gate, second_up, second_down)


def solution(mesh):
    placed = (
        P("grp", "ra"),
        P("ra"),
        P("ra", "cb"),
        P("ra", "cb"),
        P("cb", "ra"),
        P("ra"),
        P("ra", "cb"),
        P("ra", "cb"),
        P("cb", "ra"),
    )
    return jax.shard_map(
        per_device, mesh=mesh, in_specs=placed, out_specs=P("grp", "ra"), check_vma=False
    )
```

profile of v0, /device:TPU:0, one launch (start us, length us, event | category | flops | bytes accessed | tf_op | source)
XLA Modules:
  0.0 194.4 jit_solution(9216063514448310554)
XLA Ops:
  6.5 0.8 convert_element_type.31
  7.4 0.5 copy-done
  7.9 1.3 convolution_bitcast_fusion.2
  9.2 0.4 convolution_bitcast_fusion.3
  9.7 1.6 copy.12
  11.5 13.6 %psum.28 = f32[128]{0:T(128)S(1)} all-reduce(f32[128]{0:T(128)S(1)} %fusion.1), channel_id=1, replica_groups=mesh['grp'=2,'ra'=4,'cb'=4] {'ra'}, use_global_device_ids=true, to_apply=%region_2.0 | all-reduce | flops 128 | bytes 1024 | tf_op jit(solution)/shard_map/psum | solution.py:19
  25.1 22.5 %reduce-scatter.7.cloned.1.call-done = f32[352,256]{1,0:T(8,128)} async-done(((f32[1408,256]{1,0:T(8,128)}), f32[352,256]{1,0:T(8,128)}) %reduce-scatter.7.cloned.1.call-update) | async-done | bytes 360464
  47.6 1.7 fusion.14
  49.4 1.1 copy.17
  50.8 15.0 %all_gather.6 = bf16[1408,128]{1,0:T(8,128)(2,1)S(1)} all-gather(bf16[352,128]{1,0:T(8,128)(2,1)S(1)} %copy.10), channel_id=1, replica_groups=mesh['grp'=2,'ra'=4,'cb'=4] {'ra'}, dimensions={0}, use_global_device_ids=true | all-gather | bytes 450560 | tf_op jit(solution)/shard_map/all_gather | solution.py:25
  65.8 1.1 fusion.15
  67.0 30.7 %all-reduce.3.cloned.1.call-done = f32[128,512]{1,0:T(8,128)} async-done(((f32[128,512]{1,0:T(8,128)}), f32[128,512]{1,0:T(8,128)}) %all-reduce.3.cloned.1.call-update) | async-done | bytes 262160 | tf_op jit(solution)/shard_map/psum | solution.py:30
  97.7 1.1 fusion.5
  98.8 1.7 convolution_bitcast_fusion
  100.5 0.4 convolution_bitcast_fusion.1
  101.0 1.6 copy.14
  102.6 12.1 %psum.30 = f32[128]{0:T(128)S(1)} all-reduce(f32[128]{0:T(128)S(1)} %get-tuple-element.5), channel_id=1, replica_groups=mesh['grp'=2,'ra'=4,'cb'=4] {'ra'}, use_global_device_ids=true, to_apply=%region_6.7 | all-reduce | flops 128 | bytes 1024 | tf_op jit(solution)/shard_map/psum | solution.py:19
  114.7 21.5 %reduce-scatter.9.cloned.1.call-done = f32[352,256]{1,0:T(8,128)} async-done(((f32[1408,256]{1,0:T(8,128)}), f32[352,256]{1,0:T(8,128)}) %reduce-scatter.9.cloned.1.call-update) | async-done | bytes 360464
  136.2 1.7 fusion.13
  138.0 1.1 copy.19
  139.3 15.1 %all_gather.7 = bf16[1408,128]{1,0:T(8,128)(2,1)S(1)} all-gather(bf16[352,128]{1,0:T(8,128)(2,1)S(1)} %copy.11), channel_id=1, replica_groups=mesh['grp'=2,'ra'=4,'cb'=4] {'ra'}, dimensions={0}, use_global_device_ids=true | all-gather | bytes 450560 | tf_op jit(solution)/shard_map/all_gather | solution.py:25
  154.4 1.1 fusion.16
  155.5 30.7 %all-reduce.5.cloned.1.call-done = f32[128,512]{1,0:T(8,128)} async-done(((f32[128,512]{1,0:T(8,128)}), f32[128,512]{1,0:T(8,128)}) %all-reduce.5.cloned.1.call-update) | async-done | bytes 262160 | tf_op jit(solution)/shard_map/psum | solution.py:30
  186.2 1.6 fusion.7
  (33 shorter events, 1.3 us)
Async XLA Ops:
  6.5 1.4 copy-start
  6.5 2.7 %copy-start.1 = (bf16[128,512]{1,0:T(8,128)(2,1)S(1)}, bf16[128,512]{1,0:T(8,128)(2,1)}, u32[]{:S(2)}) copy-start(bf16[128,512]{1,0:T(8,128)(2,1)} %param.9) | copy-start | bytes 393220
  6.5 2.7 %copy-start.2 = (bf16[512,1408]{1,0:T(8,128)(2,1)S(1)}, bf16[512,1408]{1,0:T(8,128)(2,1)}, u32[]{:S(2)}) copy-start(bf16[512,1408]{1,0:T(8,128)(2,1)} %param.11) | copy-start | bytes 4325380
  6.5 41.1 %reduce-scatter.7.cloned.1.call-start = ((), (), s32[]{:S(2)}) async-start(), calls=%async_computation.4 | async-start | bytes 1802240
  11.3 54.5 %copy-start.3 = (bf16[1408,512]{1,0:T(8,128)(2,1)S(1)}, bf16[1408,512]{1,0:T(8,128)(2,1)}, u32[]{:S(2)}) copy-start(bf16[1408,512]{1,0:T(8,128)(2,1)} %param.13) | copy-start | bytes 4325380
  11.3 86.4 %all-reduce.3.cloned.1.call-start = ((), (), s32[]{:S(2)}) async-start(), calls=%async_computation.2 | async-start | bytes 524288 | tf_op jit(solution)/shard_map/psum | solution.py:30
  50.6 16.3 %copy-start.6 = (bf16[512]{0:T(512)(128)(2,1)S(1)}, bf16[512]{0:T(512)(128)(2,1)}, u32[]{:S(2)}) copy-start(bf16[512]{0:T(512)(128)(2,1)} %param.14) | copy-start | bytes 3076
  66.9 33.6 %copy-start.4 = (bf16[512,1408]{1,0:T(8,128)(2,1)S(1)}, bf16[512,1408]{1,0:T(8,128)(2,1)}, u32[]{:S(2)}) copy-start(bf16[512,1408]{1,0:T(8,128)(2,1)} %param.15) | copy-start | bytes 4325380
  66.9 69.3 %reduce-scatter.9.cloned.1.call-start = ((), (), s32[]{:S(2)}) async-start(), calls=%async_computation.5 | async-start | bytes 1802240
  102.6 51.8 %copy-start.5 = (bf16[1408,512]{1,0:T(8,128)(2,1)S(1)}, bf16[1408,512]{1,0:T(8,128)(2,1)}, u32[]{:S(2)}) copy-start(bf16[1408,512]{1,0:T(8,128)(2,1)} %param.17) | copy-start | bytes 4325380
  102.6 83.6 %all-reduce.5.cloned.1.call-start = ((), (), s32[]{:S(2)}) async-start(), calls=%async_computation.3 | async-start | bytes 524288 | tf_op jit(solution)/shard_map/psum | solution.py:30
Sparse Core Ops, SparseCore 0:
  11.4 36.1 reduce-scatter.6
  67.0 30.5 all-reduce.2
  102.7 33.4 reduce-scatter.8
  155.7 30.5 all-reduce.4
where the time goes:
time: 195 us; the launch traced here: 194 us
  waiting for transfers between devices  105 us (54%)
  blocking collectives  55.8 us (29%)
  between operations  13.3 us (7%)
  local copies, waits for them, and re-layouts  9.67 us (5%)
  matrix products  6.01 us (3%)
  other arithmetic  4.14 us (2%)
    psum x2, waiting for transfers between devices, sublayer(): branch = lax.psum(partial_value, 'cb')  61.4 us
    unnamed x6, waiting for transfers between devices  44 us
    all_gather x2, blocking collectives, sublayer(): lax.all_gather(hidden_t, 'ra', axis=0, tiled=True)  30.1 us
    psum x2, blocking collectives, sublayer(): total_sq = lax.psum(squares, 'ra')  25.7 us
    unnamed x20, local copies, waits for them, and re-layouts  6.04 us
  transfers between devices with their start and end apart: 4, of which 4 were waited for; matrix products, arithmetic and copies ran while one was open for 0% of the time, Pallas kernels for 0%

commit v1 on v0

--- a/solution.py
+++ b/solution.py
@@ -27,7 +27,9 @@
         (((0,), (0,)), ((), ())),
         preferred_element_type=jnp.float32,
     )
-    branch = lax.psum(partial_value, "cb")
+    branch = partial_value
+    for hop in (1, 2):
+        branch = branch + lax.ppermute(branch, "cb", [(dev, dev ^ hop) for dev in range(4)])
     return (0.5 * xf + 0.5 * branch).astype(jnp.bfloat16)
 
 

time: 195 us -> 147 us (0.75)
  waiting for transfers between devices: 105 us -> 62.1 us
  starting transfers between devices: 0.13 us -> 3.33 us
  blocking collectives: 55.8 us -> 52.7 us
  matrix products: 6.01 us -> 3.24 us
    psum x2 -> x0, waiting for transfers between devices: 61.4 us -> none  [sublayer(): branch = lax.psum(partial_value, 'cb')]
    ppermute x0 -> x4, waiting for transfers between devices: none -> 16.7 us  [sublayer(): lax.ppermute(branch, 'cb', [(dev, dev ^ hop) for dev in range(4)])]
    ppermute x0 -> x4, starting transfers between devices: none -> 3.29 us  [sublayer(): lax.ppermute(branch, 'cb', [(dev, dev ^ hop) for dev in range(4)])]
    psum x2, blocking collectives: 25.7 us -> 22.7 us  [sublayer(): total_sq = lax.psum(squares, 'ra')]
    unnamed x6 -> x4, waiting for transfers between devices: 44 us -> 45.4 us
    unnamed x20 -> x22, local copies, waits for them, and re-layouts: 6.04 us -> 6.07 us
  transfers between devices with their start and end apart: 4 -> 6, of which waited for: 4 -> 6; matrix products, arithmetic and copies ran while one was open for 0% -> 0% of each run, Pallas kernels for 0% -> 0%
where the time goes in v1:
time: 147 us
  waiting for transfers between devices  62.1 us (42%)
  blocking collectives  52.7 us (36%)
  between operations  13.6 us (9%)
  local copies, waits for them, and re-layouts  9.7 us (7%)
  starting transfers between devices  3.33 us (2%)
  matrix products  3.24 us (2%)
  other arithmetic  2.36 us (2%)
    unnamed x4, waiting for transfers between devices  45.4 us
    all_gather x2, blocking collectives, sublayer(): lax.all_gather(hidden_t, 'ra', axis=0, tiled=True)  30 us
    psum x2, blocking collectives, sublayer(): total_sq = lax.psum(squares, 'ra')  22.7 us
    ppermute x4, waiting for transfers between devices, sublayer(): lax.ppermute(branch, 'cb', [(dev, dev ^ hop) for dev in range(4)])  16.7 us
    unnamed x22, local copies, waits for them, and re-layouts  6.07 us
    slice x2, local copies, waits for them, and re-layouts, sublayer(): shares[:, :rows] * scale[None, :]  3.39 us
    ppermute x4, starting transfers between devices, sublayer(): lax.ppermute(branch, 'cb', [(dev, dev ^ hop) for dev in range(4)])  3.29 us
  transfers between devices with their start and end apart: 6, of which 6 were waited for; matrix products, arithmetic and copies ran while one was open for 0% of the time, Pallas kernels for 0%

profile of v1, /device:TPU:0, one launch (start us, length us, event | category | flops | bytes accessed | tf_op | source)
XLA Modules:
  0.0 147.0 jit_solution(14852452782660373370)
XLA Ops:
  6.5 0.8 convert_element_type.31
  7.4 0.5 copy-done
  7.9 1.3 convolution_bitcast_fusion.2
  9.7 1.6 %copy.12 = f32[1408,256]{1,0:T(8,128)} copy(f32[1408,256]{0,1:T(8,128)S(1)} %pad_maximum_fusion) | data formatting | bytes 2883584
  11.5 13.6 %psum.14 = f32[128]{0:T(128)S(1)} all-reduce(f32[128]{0:T(128)S(1)} %fusion.1), channel_id=1, replica_groups=mesh['grp'=2,'ra'=4,'cb'=4] {'ra'}, use_global_device_ids=true, to_apply=%region_2.0 | all-reduce | flops 128 | bytes 1024 | tf_op jit(solution)/shard_map/psum | solution.py:19
  25.1 22.5 %reduce-scatter.7.cloned.1.call-done = f32[352,256]{1,0:T(8,128)} async-done(((f32[1408,256]{1,0:T(8,128)}), f32[352,256]{1,0:T(8,128)}) %reduce-scatter.7.cloned.1.call-update) | async-done | bytes 360464
  47.6 1.7 %fusion.14 = (f32[352,128]{1,0:T(8,128)S(1)}, f32[352,128]{1,0:T(8,128)}) fusion(f32[352,256]{1,0:T(8,128)} %reduce-scatter.7.cloned.1.call-done), kind=kLoop, calls=%fused_computation.25 | loop fusion | bytes 720896 | tf_op jit(solution)/shard_map/slice | solution.py:22
  49.4 1.1 copy.17
  50.8 15.0 %all_gather.6 = bf16[1408,128]{1,0:T(8,128)(2,1)S(1)} all-gather(bf16[352,128]{1,0:T(8,128)(2,1)S(1)} %copy.10), channel_id=1, replica_groups=mesh['grp'=2,'ra'=4,'cb'=4] {'ra'}, dimensions={0}, use_global_device_ids=true | all-gather | bytes 450560 | tf_op jit(solution)/shard_map/all_gather | solution.py:25
  65.8 0.4 fusion.15
  66.3 1.5 %collective-permute-done = f32[128,512]{1,0:T(8,128)S(1)} collective-permute-done((f32[128,512]{1,0:T(8,128)S(1)}, f32[128,512]{1,0:T(8,128)S(1)}, u32[]{:S(2)}, u32[]{:S(2)}) %collective-permute-start) | collective-permute-done | bytes 262176 | tf_op jit(solution)/shard_map/ppermute | solution.py:32
  67.8 1.6 %collective-permute-start.1 = (f32[128,512]{1,0:T(8,128)S(1)}, f32[128,512]{1,0:T(8,128)S(1)}, u32[]{:S(2)}, u32[]{:S(2)}) collective-permute-start(f32[128,512]{1,0:T(8,128)S(1)} %add.43), channel_id=1, source_target_pairs={{0,2},{1,3},{2,0},{3,1},{4,6},{5,7},{6,4},{7,5},{8,10},{9,11},{10,... | collective-permute-start | bytes 786440 | tf_op jit(solution)/shard_map/ppermute | solution.py:32
  69.4 6.8 %collective-permute-done.1 = f32[128,512]{1,0:T(8,128)S(1)} collective-permute-done((f32[128,512]{1,0:T(8,128)S(1)}, f32[128,512]{1,0:T(8,128)S(1)}, u32[]{:S(2)}, u32[]{:S(2)}) %collective-permute-start.1) | collective-permute-done | bytes 262176 | tf_op jit(solution)/shard_map/ppermute | solution.py:32
  77.3 1.6 %copy.14 = f32[1408,256]{1,0:T(8,128)} copy(f32[1408,256]{0,1:T(8,128)S(1)} %pad_maximum_fusion.1) | data formatting | bytes 2883584
  78.9 9.0 %psum.15 = f32[128]{0:T(128)S(1)} all-reduce(f32[128]{0:T(128)S(1)} %get-tuple-element.5), channel_id=1, replica_groups=mesh['grp'=2,'ra'=4,'cb'=4] {'ra'}, use_global_device_ids=true, to_apply=%region_5.6 | all-reduce | flops 128 | bytes 1024 | tf_op jit(solution)/shard_map/psum | solution.py:19
  87.9 22.8 %reduce-scatter.9.cloned.1.call-done = f32[352,256]{1,0:T(8,128)} async-done(((f32[1408,256]{1,0:T(8,128)}), f32[352,256]{1,0:T(8,128)}) %reduce-scatter.9.cloned.1.call-update) | async-done | bytes 360464
  110.8 1.7 %fusion.13 = (f32[352,128]{1,0:T(8,128)S(1)}, f32[352,128]{1,0:T(8,128)}) fusion(f32[352,256]{1,0:T(8,128)} %reduce-scatter.9.cloned.1.call-done), kind=kLoop, calls=%fused_computation.24 | loop fusion | bytes 720896 | tf_op jit(solution)/shard_map/slice | solution.py:22
  112.6 1.1 copy.19
  113.9 15.0 %all_gather.7 = bf16[1408,128]{1,0:T(8,128)(2,1)S(1)} all-gather(bf16[352,128]{1,0:T(8,128)(2,1)S(1)} %copy.11), channel_id=1, replica_groups=mesh['grp'=2,'ra'=4,'cb'=4] {'ra'}, dimensions={0}, use_global_device_ids=true | all-gather | bytes 450560 | tf_op jit(solution)/shard_map/all_gather | solution.py:25
  129.0 0.4 fusion.16
  129.5 1.5 %collective-permute-done.2 = f32[128,512]{1,0:T(8,128)S(1)} collective-permute-done((f32[128,512]{1,0:T(8,128)S(1)}, f32[128,512]{1,0:T(8,128)S(1)}, u32[]{:S(2)}, u32[]{:S(2)}) %collective-permute-start.2) | collective-permute-done | bytes 262176 | tf_op jit(solution)/shard_map/ppermute | solution.py:32
  131.0 1.6 %collective-permute-start.3 = (f32[128,512]{1,0:T(8,128)S(1)}, f32[128,512]{1,0:T(8,128)S(1)}, u32[]{:S(2)}, u32[]{:S(2)}) collective-permute-start(f32[128,512]{1,0:T(8,128)S(1)} %add.48), channel_id=1, source_target_pairs={{0,2},{1,3},{2,0},{3,1},{4,6},{5,7},{6,4},{7,5},{8,10},{9,11},{10,... | collective-permute-start | bytes 786440 | tf_op jit(solution)/shard_map/ppermute | solution.py:32
  132.6 6.8 %collective-permute-done.3 = f32[128,512]{1,0:T(8,128)S(1)} collective-permute-done((f32[128,512]{1,0:T(8,128)S(1)}, f32[128,512]{1,0:T(8,128)S(1)}, u32[]{:S(2)}, u32[]{:S(2)}) %collective-permute-start.3) | collective-permute-done | bytes 262176 | tf_op jit(solution)/shard_map/ppermute | solution.py:32
  139.4 0.7 fusion.7
  (39 shorter events, 2.7 us)
Async XLA Ops:
  6.5 1.4 copy-start
  6.5 2.7 %copy-start.1 = (bf16[128,512]{1,0:T(8,128)(2,1)S(1)}, bf16[128,512]{1,0:T(8,128)(2,1)}, u32[]{:S(2)}) copy-start(bf16[128,512]{1,0:T(8,128)(2,1)} %param.9) | copy-start | bytes 393220
  6.5 2.7 %copy-start.2 = (bf16[512,1408]{1,0:T(8,128)(2,1)S(1)}, bf16[512,1408]{1,0:T(8,128)(2,1)}, u32[]{:S(2)}) copy-start(bf16[512,1408]{1,0:T(8,128)(2,1)} %param.11) | copy-start | bytes 4325380
  6.5 41.1 %reduce-scatter.7.cloned.1.call-start = ((), (), s32[]{:S(2)}) async-start(), calls=%async_computation.2 | async-start | bytes 1802240
  11.3 54.5 %copy-start.3 = (bf16[1408,512]{1,0:T(8,128)(2,1)S(1)}, bf16[1408,512]{1,0:T(8,128)(2,1)}, u32[]{:S(2)}) copy-start(bf16[1408,512]{1,0:T(8,128)(2,1)} %param.13) | copy-start | bytes 4325380
  11.3 99.5 %reduce-scatter.9.cloned.1.call-start = ((), (), s32[]{:S(2)}) async-start(), calls=%async_computation.3 | async-start | bytes 1802240
  65.8 3.6 %copy-start.7 = (bf16[512]{0:T(512)(128)(2,1)S(1)}, bf16[512]{0:T(512)(128)(2,1)}, u32[]{:S(2)}) copy-start(bf16[512]{0:T(512)(128)(2,1)} %param.14) | copy-start | bytes 3076
  65.8 10.6 %copy-start.4 = (bf16[512,1408]{1,0:T(8,128)(2,1)S(1)}, bf16[512,1408]{1,0:T(8,128)(2,1)}, u32[]{:S(2)}) copy-start(bf16[512,1408]{1,0:T(8,128)(2,1)} %param.16) | copy-start | bytes 4325380
  66.2 1.6 %collective-permute-start = (f32[128,512]{1,0:T(8,128)S(1)}, f32[128,512]{1,0:T(8,128)S(1)}, u32[]{:S(2)}, u32[]{:S(2)}) collective-permute-start(f32[128,512]{1,0:T(8,128)S(1)} %fusion.15), channel_id=1, source_target_pairs={{0,1},{1,0},{2,3},{3,2},{4,5},{5,4},{6,7},{7,6},{8,9},{9,8},{10,11... | collective-permute-start | bytes 786440 | tf_op jit(solution)/shard_map/ppermute | solution.py:32
  67.8 8.4 %collective-permute-start.1 = (f32[128,512]{1,0:T(8,128)S(1)}, f32[128,512]{1,0:T(8,128)S(1)}, u32[]{:S(2)}, u32[]{:S(2)}) collective-permute-start(f32[128,512]{1,0:T(8,128)S(1)} %add.43), channel_id=1, source_target_pairs={{0,2},{1,3},{2,0},{3,1},{4,6},{5,7},{6,4},{7,5},{8,10},{9,11},{10,... | collective-permute-start | bytes 786440 | tf_op jit(solution)/shard_map/ppermute | solution.py:32
  69.4 7.4 %copy-start.5 = (bf16[512,1408]{1,0:T(8,128)(2,1)S(1)}, bf16[512,1408]{1,0:T(8,128)(2,1)}, u32[]{:S(2)}) copy-start(bf16[512,1408]{1,0:T(8,128)(2,1)} %param.15) | copy-start | bytes 4325380
  78.9 50.1 %copy-start.6 = (bf16[1408,512]{1,0:T(8,128)(2,1)S(1)}, bf16[1408,512]{1,0:T(8,128)(2,1)}, u32[]{:S(2)}) copy-start(bf16[1408,512]{1,0:T(8,128)(2,1)} %param.17) | copy-start | bytes 4325380
  129.4 1.6 %collective-permute-start.2 = (f32[128,512]{1,0:T(8,128)S(1)}, f32[128,512]{1,0:T(8,128)S(1)}, u32[]{:S(2)}, u32[]{:S(2)}) collective-permute-start(f32[128,512]{1,0:T(8,128)S(1)} %fusion.16), channel_id=1, source_target_pairs={{0,1},{1,0},{2,3},{3,2},{4,5},{5,4},{6,7},{7,6},{8,9},{9,8},{10,11... | collective-permute-start | bytes 786440 | tf_op jit(solution)/shard_map/ppermute | solution.py:32
  131.0 8.4 %collective-permute-start.3 = (f32[128,512]{1,0:T(8,128)S(1)}, f32[128,512]{1,0:T(8,128)S(1)}, u32[]{:S(2)}, u32[]{:S(2)}) collective-permute-start(f32[128,512]{1,0:T(8,128)S(1)} %add.48), channel_id=1, source_target_pairs={{0,2},{1,3},{2,0},{3,1},{4,6},{5,7},{6,4},{7,5},{8,10},{9,11},{10,... | collective-permute-start | bytes 786440 | tf_op jit(solution)/shard_map/ppermute | solution.py:32
Sparse Core Ops, SparseCore 0:
  11.4 36.1 reduce-scatter.6
  79.0 31.7 reduce-scatter.8
